TPU v7x, 128 devices: a 2x2x16 block of a 8x8x16 slice. The times are simulated.
128 devices in a mesh: grp: 4 (over y, x), tp: 32 (over z, core).
Axes of the slice: x: 2, y: 2, z: 16, core: 2. Of those that a mesh axis runs over, the one named last changes fastest.
The devices are a block of a 8x8x16 slice.
Arguments:
- tokens: bfloat16 [4096, 2048], P('grp', 'tp'), parts along dimension 0, may hold values from -8 to 8
- carried: float32 [2, 2, 32, 64, 4096], P(None, None, 'tp', None, 'grp'), parts along dimension 4, may hold values from -3 to 3
- proj_in: bfloat16 [2, 2048, 512], P(None, None, 'tp'), may hold values from -0.125 to 0.125
- proj_gate: bfloat16 [2, 2048, 512], P(None, None, 'tp'), may hold values from -0.125 to 0.125
- proj_out: bfloat16 [2, 512, 2048], P(None, None, 'tp'), may hold values from -0.5 to 0.5
- norm_params: bfloat16 [2, 2, 2048], P(None, None, 'tp'), may hold values from -0.5 to 2.4
- lambda_re: float32 [2, 32, 64], P(None, 'tp'), may hold values from -1 to -0.05
- lambda_im: float32 [2, 32, 64], P(None, 'tp'), may hold values from -3 to 3
- log_step: float32 [2, 32], P(None, 'tp'), may hold values from -3 to 0
- in_coupling: float32 [2, 2, 32, 64, 16], P(None, None, 'tp'), may hold values from -1 to 1
- out_coupling: float32 [2, 2, 32, 16, 64], P(None, None, 'tp'), may hold values from -1.5 to 1.5
- skip_gain: float32 [2, 512], P(None, 'tp'), may hold values from -4 to 4
Outputs:
- stream_out: bfloat16 [4096, 2048], P('grp', 'tp'), parts along dimension 0
- new_carried: float32 [2, 2, 32, 64, 4096], P(None, None, 'tp', None, 'grp'), parts along dimension 4
There are 4 independent parts, one for each index of `grp`. A program takes and returns all parts, laid end to end along the dimension named above; an argument that names none is the same for every part. Nothing has to cross between parts.
All inputs are finite; a program needn't handle non-finite values.
Results may differ from a plain program's by a relative error of at most 0.015.
Values may be sent and summed in bfloat16 or wider, within the bound.
A program may use at most 64 MiB of HBM per device.

v0:
```python
import jax
import jax.numpy as jnp
from jax import lax
from jax.sharding import Mesh
from jax.sharding import PartitionSpec as P

TP = ("tp_0", "tp_1")
residual_scale = 1.4142135623730951
norm_eps = 1e-05


def gather_turned(arrays, axis, dims):
    turned = [jnp.moveaxis(a, dim, 0) for a, dim in zip(arrays, dims)]
    both = jnp.concatenate([t.reshape(len(t), -1) for t in turned], axis=1)
    out, at, finished = (lax.all_gather(both, axis, axis=0, tiled=True), 0, [])
    for t, dim in zip(turned, dims):
        piece = out[:, at : at + t[0].size].reshape(-1, *t.shape[1:])
        finished.append(jnp.moveaxis(piece, 0, dim))
        at += t[0].size
    return tuple(finished)


def in_order(tiles, dim):
    tiles = jnp.moveaxis(tiles, 0, dim)
    shape = tiles.shape
    return tiles.reshape(*shape[:dim], shape[dim] * shape[dim + 1], *shape[dim + 2 :])


def all_blocks(array, axes, sequence):
    tiles = array
    for k in sequence:
        tiles = lax.all_gather(tiles, axes[k])
    done = sequence[::-1]
    back = [done.index(k) for k in range(len(axes))]
    tiles = tiles.transpose(*back, *range(len(axes), tiles.ndim))
    return tiles.reshape(-1, *array.shape)


def gather_axes(array, axes, sequence, dim):
    return in_order(all_blocks(array, axes, sequence), dim)


def discretize(lam_re, lam_im, log_dt, coupling):
    step_len = jnp.exp(log_dt)[:, None]
    modulus = jnp.exp(lam_re * step_len)
    decay_re = modulus * jnp.cos(lam_im * step_len)
    decay_im = modulus * jnp.sin(lam_im * step_len)
    denominator = lam_re * lam_re + lam_im * lam_im
    shifted = decay_re - 1.0
    coef_re = (shifted * lam_re + decay_im * lam_im) / denominator
    coef_im = (decay_im * lam_re - shifted * lam_im) / denominator
    in_re = coef_re[..., None] * coupling[0] - coef_im[..., None] * coupling[1]
    in_im = coef_re[..., None] * coupling[1] + coef_im[..., None] * coupling[0]
    return (decay_re, decay_im, in_re, in_im)


def recur(drive, gate_pre, states, lam_re, lam_im, log_dt, in_c, output_coupling, skip_connection):
    channel_groups = lam_re.shape[0]
    batch_rows = drive.shape[0]
    drive_expanded = drive.astype(jnp.float32).reshape(batch_rows, channel_groups, -1)
    decay_re, decay_im, in_re, in_im = discretize(lam_re, lam_im, log_dt, in_c)
    push_re = jnp.einsum("bgc,gpc->gpb", drive_expanded, in_re)
    push_im = jnp.einsum("bgc,gpc->gpb", drive_expanded, in_im)
    fresh_real = decay_re[..., None] * states[0] - decay_im[..., None] * states[1] + push_re
    fresh_imaginary = decay_re[..., None] * states[1] + decay_im[..., None] * states[0] + push_im
    readout_rows = (
        jnp.einsum("jyn,jmy->njm", fresh_real, output_coupling[0])
        - jnp.einsum("jyn,jmy->njm", fresh_imaginary, output_coupling[1])
        + skip_connection.reshape(channel_groups, -1) * drive_expanded
    )
    readout_rows = readout_rows.reshape(batch_rows, -1)
    gated = (jax.nn.gelu(readout_rows) * jax.nn.sigmoid(gate_pre.astype(jnp.float32))).astype(
        jnp.bfloat16
    )
    return (gated, jnp.stack([fresh_real, fresh_imaginary]))


def norm_whole(summed, params):
    wide = summed.astype(jnp.float32)
    mean_row = jnp.mean(wide, axis=-1, keepdims=True)
    var_row = jnp.mean(wide * wide, axis=-1, keepdims=True) - mean_row * mean_row
    scaled = (wide - mean_row) * lax.rsqrt(var_row + norm_eps)
    return (scaled * params[0].astype(jnp.float32) + params[1].astype(jnp.float32)).astype(
        jnp.bfloat16
    )


def per_device(
    tokens,
    carried,
    proj_in,
    proj_gate,
    proj_out,
    norm_params,
    lambda_re,
    lambda_im,
    log_step,
    in_coupling,
    out_coupling,
    skip_gain,
):
    layer_count = proj_in.shape[0]
    width_dev = tokens.shape[1]
    out_whole, params_whole = gather_turned((proj_out, norm_params), TP, (2, 2))
    whole_rows = lax.all_gather(tokens, TP, axis=1, tiled=True)
    new_states = []
    for layer_idx in range(layer_count):
        drive = jnp.dot(whole_rows, proj_in[layer_idx], preferred_element_type=jnp.float32).astype(
            jnp.bfloat16
        )
        gate_pre = jnp.dot(
            whole_rows, proj_gate[layer_idx], preferred_element_type=jnp.float32
        ).astype(jnp.bfloat16)
        gated, states = recur(
            drive,
            gate_pre,
            carried[layer_idx],
            lambda_re[layer_idx],
            lambda_im[layer_idx],
            log_step[layer_idx],
            in_coupling[layer_idx],
            out_coupling[layer_idx],
            skip_gain[layer_idx],
        )
        gated_all = gather_axes(gated, TP, (0, 1), 1)
        mixed = jnp.dot(gated_all, out_whole[layer_idx], preferred_element_type=jnp.float32)
        summed = (residual_scale * whole_rows.astype(jnp.float32) + mixed).astype(jnp.bfloat16)
        whole_rows = norm_whole(summed, params_whole[layer_idx])
        new_states.append(states)
    own_cols = lax.dynamic_slice_in_dim(whole_rows, lax.axis_index(TP) * width_dev, width_dev, 1)
    return (own_cols, jnp.stack(new_states))


def solution(mesh):
    finer = Mesh(mesh.devices.reshape(mesh.shape["grp"], 16, 2), ("grp", "tp_0", "tp_1"))
    return jax.shard_map(
        per_device,
        mesh=finer,
        in_specs=(
            P("grp", TP),
            P(None, None, TP, None, "grp"),
            P(None, None, TP),
            P(None, None, TP),
            P(None, None, TP),
            P(None, None, TP),
            P(None, TP, None),
            P(None, TP, None),
            P(None, TP),
            P(None, None, TP, None, None),
            P(None, None, TP, None, None),
            P(None, TP),
        ),
        out_specs=(P("grp", TP), P(None, None, TP, None, "grp")),
        check_vma=False,
    )
```

profile of v0, /device:TPU:69, one launch (start us, length us, event | category | flops | bytes accessed | tf_op | source)
XLA Modules:
  0.0 249.1 jit_solution(6978325671678053711)
XLA Ops:
  7.3 0.7 all-gather.9.cloned.1.call-update
  8.1 0.8 copy.43
  8.9 0.9 copy.54
  9.8 0.7 pad_maximum_fusion
  10.6 1.3 fusion.103
  13.3 0.8 slice_bitcast_fusion.4
  14.0 0.7 fusion.91
  14.8 0.8 fusion.97
  15.5 0.7 fusion.100
  16.2 71.2 %all-gather.9.cloned.1.call-done = bf16[1024,2048]{0,1:T(8,128)(2,1)} async-done(((bf16[1024,64]{0,1:T(8,128)(2,1)}), bf16[1024,2048]{0,1:T(8,128)(2,1)}) %all-gather.9.cloned.1.call-update) | async-done | bytes 4194320 | tf_op jit(solution)/shard_map/all_gather | solution.py:105
  87.4 3.0 %convolution_convert_fusion.1 = bf16[1024,16]{0,1:T(8,128)(2,1)S(1)} fusion(bf16[1024,2048]{0,1:T(8,128)(2,1)} %all-gather.9.cloned.1.call-done, bf16[2,2048,16]{1,2,0:T(8,128)(2,1)} %param.14), kind=kOutput, calls=%fused_computation.33 | convolution fusion | flops 67125248 | bytes 4292608 | tf_op jit(solution)/shard_map/dot_general | solution.py:108
  91.2 0.7 fusion.25
  91.9 27.8 %all-gather = bf16[16384,16]{0,1:T(8,128)(2,1)S(1)} all-gather(bf16[1024,16]{0,1:T(8,128)(2,1)S(1)} %fusion.25), channel_id=2, replica_groups=mesh['grp'=4,'tp_0'=16,'tp_1'=2] {'tp_0'}, dimensions={0}, use_global_device_ids=true | all-gather | bytes 557056 | tf_op jit(solution)/shard_map/all_gather | solution.py:32
  119.7 0.8 copy.58
  120.7 6.6 %copy.39 = bf16[1024,2048]{1,0:T(8,128)(2,1)} copy(bf16[1024,2048]{0,1:T(8,128)(2,1)} %all-gather.9.cloned.1.call-done) | data formatting | bytes 8388608 | tf_op jit(solution)/shard_map/all_gather | solution.py:105
  127.2 30.5 %all-gather.11.cloned.1.call-done = bf16[2048,1028]{1,0:T(8,128)(2,1)} async-done(((bf16[64,1028]{1,0:T(8,128)(2,1)}), bf16[2048,1028]{1,0:T(8,128)(2,1)}) %all-gather.11.cloned.1.call-update) | async-done | bytes 4210704 | tf_op jit(solution)/shard_map/all_gather | solution.py:15
  157.7 1.1 slice.178
  159.0 4.7 %slice.176 = bf16[2048,1024]{1,0:T(8,128)(2,1)} slice(bf16[2048,1028]{1,0:T(8,128)(2,1)} %all-gather.11.cloned.1.call-done), slice={[0:2048], [0:1024]} | slice | bytes 8388608 | tf_op jit(solution)/shard_map/slice | solution.py:17
  163.7 6.6 %copy.51 = bf16[2048,1024]{0,1:T(8,128)(2,1)} copy(bf16[2048,1024]{1,0:T(8,128)(2,1)} %slice.176) | data formatting | bytes 8388608 | tf_op jit(solution)/shard_map/reshape | solution.py:17
  170.3 3.0 %all-gather.13.cloned.1.call-done = bf16[32,1024,16]{1,2,0:T(8,128)(2,1)} async-done(((bf16[16,1024,16]{1,2,0:T(8,128)(2,1)}), bf16[32,1024,16]{1,2,0:T(8,128)(2,1)}) %all-gather.13.cloned.1.call-update) | async-done | bytes 1048592 | tf_op jit(solution)/shard_map/all_gather | solution.py:32
  173.3 1.3 copy.41
  174.6 6.0 %convert_reduce_fusion = (f32[1024]{0:T(1024)S(1)}, f32[1024]{0:T(1024)S(1)}, bf16[1024,2048]{1,0:T(8,128)(2,1)S(1)}) fusion(bf16[1024,512]{0,1:T(8,128)(2,1)S(1)} %bitcast.323, bf16[2,512,2048]{2,1,0:T(8,128)(2,1)} %bitcast.310, bf16[1024,2048]{1,0:T(8,128)(2,1)} %copy.39), kind=kOutput, calls=%fused_computation.2 | convolution fusion | flops 2164258816 | bytes 11542528 | tf_op jit(solution)/shard_map/dot_general | solution.py:126
  180.6 1.9 fusion.3
  182.5 1.2 convolution_convert_fusion.3
  184.4 1.2 fusion.24
  185.7 25.7 %all-gather.2 = bf16[16384,16]{0,1:T(8,128)(2,1)S(1)} all-gather(bf16[1024,16]{0,1:T(8,128)(2,1)S(1)} %fusion.24), channel_id=4, replica_groups=mesh['grp'=4,'tp_0'=16,'tp_1'=2] {'tp_0'}, dimensions={0}, use_global_device_ids=true | all-gather | bytes 557056 | tf_op jit(solution)/shard_map/all_gather | solution.py:32
  211.4 0.8 copy.57
  212.5 1.1 maximum_bitcast_fusion
  213.6 20.3 %all-gather.15.cloned.1.call-done = bf16[32,1024,16]{1,2,0:T(8,128)(2,1)} async-done(((bf16[16,1024,16]{1,2,0:T(8,128)(2,1)}), bf16[32,1024,16]{1,2,0:T(8,128)(2,1)}) %all-gather.15.cloned.1.call-update) | async-done | bytes 1048592 | tf_op jit(solution)/shard_map/all_gather | solution.py:32
  233.9 1.3 copy.47
  235.2 6.1 %fusion.102 = (f32[1024]{0:T(1024)S(1)}, f32[1024]{0:T(1024)S(1)}, f32[1024,2048]{1,0:T(8,128)S(1)}) fusion(bf16[1024,512]{0,1:T(8,128)(2,1)S(1)} %bitcast.322, bf16[2,512,2048]{2,1,0:T(8,128)(2,1)} %bitcast.311, bf16[1024,2048]{1,0:T(8,128)(2,1)} %copy-done), kind=kOutput, calls=%fused_computation.171 | convolution fusion | flops 2164258816 | bytes 15736832 | tf_op jit(solution)/shard_map/dot_general | solution.py:126
  241.8 0.8 copy.49
  (39 shorter events, 2.9 us)
Async XLA Ops:
  7.2 83.2 %copy-start.5 = (f32[2,2,1,64,16]{3,4,2,1,0:T(8,128)S(1)}, f32[2,2,1,64,16]{3,4,2,1,0:T(8,128)}, u32[]{:S(2)}) copy-start(f32[2,2,1,64,16]{3,4,2,1,0:T(8,128)} %param.21) | copy-start | bytes 49156
  7.2 83.2 %copy-start.2 = (f32[2,2,1,64,1024]{4,3,2,1,0:T(8,128)S(1)}, f32[2,2,1,64,1024]{4,3,2,1,0:T(8,128)}, u32[]{:S(2)}) copy-start(f32[2,2,1,64,1024]{4,3,2,1,0:T(8,128)} %param.13) | copy-start | bytes 3145732
  7.2 83.4 %copy-start.6 = (f32[2,2,1,16,64]{4,3,2,1,0:T(8,128)S(1)}, f32[2,2,1,16,64]{4,3,2,1,0:T(8,128)}, u32[]{:S(2)}) copy-start(f32[2,2,1,16,64]{4,3,2,1,0:T(8,128)} %param.22) | copy-start | bytes 49156
  7.2 84.0 %copy-start.3 = (bf16[2,2048,16]{1,2,0:T(8,128)(2,1)S(1)}, bf16[2,2048,16]{1,2,0:T(8,128)(2,1)}, u32[]{:S(2)}) copy-start(bf16[2,2048,16]{1,2,0:T(8,128)(2,1)} %param.15) | copy-start | bytes 393220
  7.2 80.2 %all-gather.9.cloned.1.call-start = ((), (), s32[]{:S(2)}) async-start(), calls=%async_computation | async-start | bytes 4325376 | tf_op jit(solution)/shard_map/all_gather | solution.py:105
  8.0 149.7 %all-gather.11.cloned.1.call-start = ((), (), s32[]{:S(2)}) async-start(), calls=%async_computation.1 | async-start | bytes 4866048 | tf_op jit(solution)/shard_map/all_gather | solution.py:15
  10.5 162.8 %all-gather.13.cloned.1.call-start = ((), (), s32[]{:S(2)}) async-start(), calls=%async_computation.2 | async-start | bytes 1572864 | tf_op jit(solution)/shard_map/all_gather | solution.py:32
  87.4 3.8 %copy-start.1 = (bf16[1024,2048]{0,1:T(8,128)(2,1)S(1)}, bf16[1024,2048]{0,1:T(8,128)(2,1)}, u32[]{:S(2)}) copy-start(bf16[1024,2048]{0,1:T(8,128)(2,1)} %all-gather.9.cloned.1.call-done) | copy-start | bytes 12582916
  120.6 113.3 %all-gather.15.cloned.1.call-start = ((), (), s32[]{:S(2)}) async-start(), calls=%async_computation.3 | async-start | bytes 1572864 | tf_op jit(solution)/shard_map/all_gather | solution.py:32
  180.6 1.9 copy-start.4
  182.5 3.2 %copy-start = (bf16[1024,2048]{1,0:T(8,128)(2,1)}, bf16[1024,2048]{1,0:T(8,128)(2,1)S(1)}, u32[]{:S(2)}) copy-start(bf16[1024,2048]{1,0:T(8,128)(2,1)S(1)} %fusion.3) | copy-start | bytes 12582916
Sparse Core Ops, SparseCore 0:
  9.8 77.5 all-gather.8
  89.1 68.5 all-gather.10
  160.0 13.2 all-gather.12
  212.4 21.4 all-gather.14
where the time goes:
time: 250 us; the launch traced here: 249 us
  waiting for transfers between devices  126 us (50%)
  blocking collectives  53.5 us (21%)
  local copies, waits for them, and re-layouts  28.1 us (11%)
  matrix products  19.6 us (8%)
  between operations  15.4 us (6%)
  other arithmetic  6.37 us (3%)
    all_gather x1, waiting for transfers between devices, per_device(): whole_rows = lax.all_gather(tokens, TP, axis=1, tiled=True)  71.2 us
    all_gather x2, blocking collectives, all_blocks(): tiles = lax.all_gather(tiles, axes[k])  53.5 us
    all_gather x1, waiting for transfers between devices, gather_turned(): out, at, finished = (lax.all_gather(both, axis, axis=0, tiled=True), 0, [])  30.5 us
    all_gather x2, waiting for transfers between devices, all_blocks(): tiles = lax.all_gather(tiles, axes[k])  23.2 us
    dot_general x2, matrix products, per_device(): jnp.dot(gated_all, out_whole[layer_idx], preferred_element_type=jnp.float32)  12.1 us
    reshape x2, local copies, waits for them, and re-layouts, gather_turned(): piece = out[:, at:at + t[0].size].reshape(-1, *t.shape[1:])  6.58 us
    all_gather x1, local copies, waits for them, and re-layouts, per_device(): whole_rows = lax.all_gather(tokens, TP, axis=1, tiled=True)  6.56 us
    slice x3, local copies, waits for them, and re-layouts, gather_turned(): piece = out[:, at:at + t[0].size].reshape(-1, *t.shape[1:])  5.98 us
  transfers between devices with their start and end apart: 4, of which 4 were waited for; matrix products, arithmetic and copies ran while one was open for 13% of the time, Pallas kernels for 0%

commit v1 on v0

--- a/solution.py
+++ b/solution.py
@@ -3,6 +3,7 @@
 from jax import lax
 from jax.sharding import Mesh
 from jax.sharding import PartitionSpec as P
+from jax.lax import all_to_all, axis_size
 
 TP = ("tp_0", "tp_1")
 residual_scale = 1.4142135623730951
@@ -102,7 +103,7 @@
     layer_count = proj_in.shape[0]
     width_dev = tokens.shape[1]
     out_whole, params_whole = gather_turned((proj_out, norm_params), TP, (2, 2))
-    whole_rows = lax.all_gather(tokens, TP, axis=1, tiled=True)
+    whole_rows = jnp.concatenate(all_to_all(jnp.stack(axis_size(TP) * [tokens]), TP, 0, 0), axis=1)
     new_states = []
     for layer_idx in range(layer_count):
         drive = jnp.dot(whole_rows, proj_in[layer_idx], preferred_element_type=jnp.float32).astype(

time: 250 us -> 370 us (1.48)
  waiting for transfers between devices: 126 us -> 226 us
  starting transfers between devices: 0.25 us -> 18.9 us
    all_to_all x0 -> x1, waiting for transfers between devices: none -> 204 us  [per_device(): all_to_all(jnp.stack(axis_size(TP) * [tokens]), TP, 0, 0)]
    all_gather x1 -> x0, waiting for transfers between devices: 71.2 us -> none  [per_device(): whole_rows = lax.all_gather(tokens, TP, axis=1, tiled=True)]
    all_gather x1, waiting for transfers between devices: 30.5 us -> 0.02 us  [gather_turned(): out, at, finished = (lax.all_gather(both, axis, axis=0, tiled=True), 0, [])]
    all_to_all x0 -> x1, starting transfers between devices: none -> 18.7 us  [per_device(): all_to_all(jnp.stack(axis_size(TP) * [tokens]), TP, 0, 0)]
    reshape x0 -> x1, local copies, waits for them, and re-layouts: none -> 6.68 us  [per_device(): jnp.concatenate(all_to_all(jnp.stack(axis_size(TP) * [tokens]), TP, 0, 0)...]
    all_gather x1 -> x0, local copies, waits for them, and re-layouts: 6.56 us -> none  [per_device(): whole_rows = lax.all_gather(tokens, TP, axis=1, tiled=True)]
  transfers between devices with their start and end apart: 4 -> 4, of which waited for: 4 -> 2; matrix products, arithmetic and copies ran while one was open for 13% -> 8% of each run, Pallas kernels for 0% -> 0%
where the time goes in v1:
time: 370 us
  waiting for transfers between devices  226 us (61%)
  blocking collectives  54.6 us (15%)
  local copies, waits for them, and re-layouts  28.7 us (8%)
  matrix products  21.6 us (6%)
  starting transfers between devices  18.9 us (5%)
  between operations  15.5 us (4%)
  other arithmetic  4.34 us (1%)
    all_to_all x1, waiting for transfers between devices, per_device(): all_to_all(jnp.stack(axis_size(TP) * [tokens]), TP, 0, 0)  204 us
    all_gather x2, blocking collectives, all_blocks(): tiles = lax.all_gather(tiles, axes[k])  54.6 us
    all_gather x2, waiting for transfers between devices, all_blocks(): tiles = lax.all_gather(tiles, axes[k])  22.4 us
    all_to_all x1, starting transfers between devices, per_device(): all_to_all(jnp.stack(axis_size(TP) * [tokens]), TP, 0, 0)  18.7 us
    dot_general x2, matrix products, per_device(): jnp.dot(gated_all, out_whole[layer_idx], preferred_element_type=jnp.float32)  12.1 us
  transfers between devices with their start and end apart: 4, of which 2 were waited for; matrix products, arithmetic and copies ran while one was open for 8% of the time, Pallas kernels for 0%

profile of v1, /device:TPU:69, one launch (start us, length us, event | category | flops | bytes accessed | tf_op | source)
XLA Modules:
  0.0 369.8 jit_solution(17411419499256291668)
XLA Ops:
  7.2 3.5 stack.20
  10.7 18.7 %all-to-all-start = ((bf16[32,1024,64]{1,2,0:T(8,128)(2,1)}), bf16[32,1024,64]{1,2,0:T(8,128)(2,1)}, u32[]{:S(2)}, u32[]{:S(2)}) async-start(bf16[32,1024,64]{1,2,0:T(8,128)(2,1)} %stack.20), calls=%async_computation | async-start | bytes 8388608 | tf_op jit(solution)/shard_map/all_to_all | solution.py:106
  29.7 0.7 pad_maximum_fusion
  30.5 0.6 fusion.103
  32.6 203.6 %all-to-all-done = bf16[32,1024,64]{1,2,0:T(8,128)(2,1)} async-done(((bf16[32,1024,64]{1,2,0:T(8,128)(2,1)}), bf16[32,1024,64]{1,2,0:T(8,128)(2,1)}, u32[]{:S(2)}, u32[]{:S(2)}) %all-to-all-start) | async-done | bytes 4194336 | tf_op jit(solution)/shard_map/all_to_all | solution.py:106
  236.2 2.8 convolution_convert_fusion.1
  239.1 0.2 convolution_add_fusion.3
  239.5 0.2 convolution_add_fusion.2
  239.7 0.2 fusion.40
  239.9 2.9 fusion.25
  242.7 29.0 %all-gather = bf16[16384,16]{0,1:T(8,128)(2,1)S(1)} all-gather(bf16[1024,16]{0,1:T(8,128)(2,1)S(1)} %fusion.25), channel_id=2, replica_groups=mesh['grp'=4,'tp_0'=16,'tp_1'=2] {'tp_0'}, dimensions={0}, use_global_device_ids=true | all-gather | bytes 557056 | tf_op jit(solution)/shard_map/all_gather | solution.py:33
  271.7 0.8 copy.58
  272.7 1.1 slice.178
  273.8 0.2 copy.45
  274.0 4.7 %slice.176 = bf16[2048,1024]{1,0:T(8,128)(2,1)} slice(bf16[2048,1028]{1,0:T(8,128)(2,1)} %all-gather.8.cloned.1.call-done), slice={[0:2048], [0:1024]} | slice | bytes 8388608 | tf_op jit(solution)/shard_map/slice | solution.py:18
  278.7 6.5 %copy.51 = bf16[2048,1024]{0,1:T(8,128)(2,1)} copy(bf16[2048,1024]{1,0:T(8,128)(2,1)} %slice.176) | data formatting | bytes 8388608 | tf_op jit(solution)/shard_map/reshape | solution.py:18
  285.3 6.7 %copy.39 = bf16[1024,2048]{1,0:T(8,128)(2,1)} copy(bf16[1024,2048]{0,1:T(8,128)(2,1)} %bitcast.1) | data formatting | bytes 8388608 | tf_op jit(solution)/shard_map/reshape | solution.py:106
  292.0 1.3 copy.41
  293.3 6.0 %convert_reduce_fusion = (f32[1024]{0:T(1024)S(1)}, f32[1024]{0:T(1024)S(1)}, bf16[1024,2048]{1,0:T(8,128)(2,1)S(1)}) fusion(bf16[1024,512]{0,1:T(8,128)(2,1)S(1)} %bitcast.326, bf16[2,512,2048]{2,1,0:T(8,128)(2,1)} %bitcast.313, bf16[1024,2048]{1,0:T(8,128)(2,1)} %copy.39), kind=kOutput, calls=%fused_computation.2 | convolution fusion | flops 2164258816 | bytes 11542528 | tf_op jit(solution)/shard_map/dot_general | solution.py:127
  299.3 1.9 fusion.3
  301.2 1.2 convolution_convert_fusion.3
  302.4 0.2 convolution_add_fusion
  302.6 0.2 convolution_add_fusion.1
  303.1 1.2 fusion.24
  304.4 25.6 %all-gather.2 = bf16[16384,16]{0,1:T(8,128)(2,1)S(1)} all-gather(bf16[1024,16]{0,1:T(8,128)(2,1)S(1)} %fusion.24), channel_id=4, replica_groups=mesh['grp'=4,'tp_0'=16,'tp_1'=2] {'tp_0'}, dimensions={0}, use_global_device_ids=true | all-gather | bytes 557056 | tf_op jit(solution)/shard_map/all_gather | solution.py:33
  329.9 0.8 copy.57
  331.1 1.1 maximum_bitcast_fusion
  332.2 22.4 %all-gather.12.cloned.1.call-done = bf16[32,1024,16]{1,2,0:T(8,128)(2,1)} async-done(((bf16[16,1024,16]{1,2,0:T(8,128)(2,1)}), bf16[32,1024,16]{1,2,0:T(8,128)(2,1)}) %all-gather.12.cloned.1.call-update) | async-done | bytes 1048592 | tf_op jit(solution)/shard_map/all_gather | solution.py:33
  354.5 1.3 copy.47
  355.8 6.1 %fusion.102 = (f32[1024]{0:T(1024)S(1)}, f32[1024]{0:T(1024)S(1)}, f32[1024,2048]{1,0:T(8,128)S(1)}) fusion(bf16[1024,512]{0,1:T(8,128)(2,1)S(1)} %bitcast.325, bf16[2,512,2048]{2,1,0:T(8,128)(2,1)} %bitcast.314, bf16[1024,2048]{1,0:T(8,128)(2,1)} %copy-done), kind=kOutput, calls=%fused_computation.171 | convolution fusion | flops 2164258816 | bytes 15736832 | tf_op jit(solution)/shard_map/dot_general | solution.py:127
  361.9 0.5 fusion.29
  362.4 0.8 copy.49
  (49 shorter events, 1.4 us)
Async XLA Ops:
  10.7 18.8 %copy-start.10 = (bf16[2,2,64]{2,1,0:T(2,128)(2,1)S(1)}, bf16[2,2,64]{2,1,0:T(2,128)(2,1)}, u32[]{:S(2)}) copy-start(bf16[2,2,64]{2,1,0:T(2,128)(2,1)} %param.17) | copy-start | bytes 1540
  10.7 19.0 %copy-start.4 = (bf16[2,512,64]{1,2,0:T(8,128)(2,1)S(1)}, bf16[2,512,64]{1,2,0:T(8,128)(2,1)}, u32[]{:S(2)}) copy-start(bf16[2,512,64]{1,2,0:T(8,128)(2,1)} %param.16) | copy-start | bytes 393220
  10.7 19.8 %copy-start.9 = (f32[2,1]{0,1:T(1,128)S(1)}, f32[2,1]{0,1:T(1,128)}, u32[]{:S(2)}) copy-start(f32[2,1]{0,1:T(1,128)} %param.20) | copy-start | bytes 28
  10.7 21.8 %copy-start.11 = (f32[2,16]{1,0:T(2,128)S(1)}, f32[2,16]{1,0:T(2,128)}, u32[]{:S(2)}) copy-start(f32[2,16]{1,0:T(2,128)} %param.23) | copy-start | bytes 388
  10.7 21.8 %copy-start.7 = (f32[2,1,64]{2,1,0:T(1,128)S(1)}, f32[2,1,64]{2,1,0:T(1,128)}, u32[]{:S(2)}) copy-start(f32[2,1,64]{2,1,0:T(1,128)} %param.19) | copy-start | bytes 1540
  10.7 21.8 %copy-start.8 = (f32[2,1,64]{2,1,0:T(1,128)S(1)}, f32[2,1,64]{2,1,0:T(1,128)}, u32[]{:S(2)}) copy-start(f32[2,1,64]{2,1,0:T(1,128)} %param.18) | copy-start | bytes 1540
  10.7 225.5 %copy-start.3 = (bf16[2,2048,16]{1,2,0:T(8,128)(2,1)S(1)}, bf16[2,2048,16]{1,2,0:T(8,128)(2,1)}, u32[]{:S(2)}) copy-start(bf16[2,2048,16]{1,2,0:T(8,128)(2,1)} %param.14) | copy-start | bytes 393220
  10.7 225.5 %all-to-all-start = ((bf16[32,1024,64]{1,2,0:T(8,128)(2,1)}), bf16[32,1024,64]{1,2,0:T(8,128)(2,1)}, u32[]{:S(2)}, u32[]{:S(2)}) async-start(bf16[32,1024,64]{1,2,0:T(8,128)(2,1)} %stack.20), calls=%async_computation | async-start | bytes 8388608 | tf_op jit(solution)/shard_map/all_to_all | solution.py:106
  29.4 209.7 %copy-start.1 = (f32[2,2,1,64,1024]{4,3,2,1,0:T(8,128)S(1)}, f32[2,2,1,64,1024]{4,3,2,1,0:T(8,128)}, u32[]{:S(2)}) copy-start(f32[2,2,1,64,1024]{4,3,2,1,0:T(8,128)} %param.13) | copy-start | bytes 3145732
  29.4 209.7 %copy-start.5 = (f32[2,2,1,64,16]{3,4,2,1,0:T(8,128)S(1)}, f32[2,2,1,64,16]{3,4,2,1,0:T(8,128)}, u32[]{:S(2)}) copy-start(f32[2,2,1,64,16]{3,4,2,1,0:T(8,128)} %param.21) | copy-start | bytes 49156
  29.4 209.9 %copy-start.6 = (f32[2,2,1,16,64]{4,3,2,1,0:T(8,128)S(1)}, f32[2,2,1,16,64]{4,3,2,1,0:T(8,128)}, u32[]{:S(2)}) copy-start(f32[2,2,1,16,64]{4,3,2,1,0:T(8,128)} %param.22) | copy-start | bytes 49156
  29.4 210.4 %copy-start.2 = (bf16[2,2048,16]{1,2,0:T(8,128)(2,1)S(1)}, bf16[2,2048,16]{1,2,0:T(8,128)(2,1)}, u32[]{:S(2)}) copy-start(bf16[2,2048,16]{1,2,0:T(8,128)(2,1)} %param.15) | copy-start | bytes 393220
  29.4 243.3 %all-gather.8.cloned.1.call-start = ((), (), s32[]{:S(2)}) async-start(), calls=%async_computation.1 | async-start | bytes 4866048 | tf_op jit(solution)/shard_map/all_gather | solution.py:16
  30.4 261.6 %all-gather.10.cloned.1.call-start = ((), (), s32[]{:S(2)}) async-start(), calls=%async_computation.2 | async-start | bytes 1572864 | tf_op jit(solution)/shard_map/all_gather | solution.py:33
  272.6 81.9 %all-gather.12.cloned.1.call-start = ((), (), s32[]{:S(2)}) async-start(), calls=%async_computation.3 | async-start | bytes 1572864 | tf_op jit(solution)/shard_map/all_gather | solution.py:33
  301.2 3.2 copy-start
Sparse Core Ops, SparseCore 0:
  32.0 155.4 all-gather.7
  272.7 18.9 all-gather.9
  331.0 23.5 all-gather.11
